TPU v7x, 128 devices: a whole 4x4x4 slice. The times are simulated.
128 devices in a mesh: rep: 2 (over z_hi), fs: 32 (over z_lo, y, x), tp: 2 (over core).
Axes of the slice: x: 4, y: 4, z: 4 (z_hi: 2, z_lo: 2; z = z_hi * 2 + z_lo), core: 2. Of those that a mesh axis runs over, the one named last changes fastest.
Arguments:
- resid: bfloat16 [65536, 2048], P(('rep', 'fs'), 'tp'), may hold values from -6 to 6
- gain_mix_in: float32 [2048], replicated, may hold values from 0.1 to 1.9
- u_weight: float32 [2048, 1024], P('fs', 'tp'), may hold values from -0.125 to 0.125
- v_weight: float32 [2048, 1024], P('fs', 'tp'), may hold values from -0.125 to 0.125
- u_scale: float32 [1024], P('tp'), may hold values from 0.5 to 2
- v_scale: float32 [1024], P('tp'), may hold values from 0.3 to 3
- v_gain: float32 [1024], P('tp'), may hold values from 0.1 to 1.9
- mix_matrix: float32 [16, 128, 128], P('tp'), may hold values from -0.5 to 0.5
- mix_bias: float32 [16, 128], P('tp'), may hold values from 0.1 to 1.9
- out_weight: float32 [1024, 2048], P('tp', 'fs'), may hold values from -0.1875 to 0.1875
- out_scale: float32 [2048], P('fs'), may hold values from 0.3 to 3
- gain_mix_out: float32 [2048], replicated, may hold values from 0.1 to 1.9
- gain_ffn_in: float32 [2048], replicated, may hold values from 0.1 to 1.9
- up_weight: float32 [2048, 4096], P('fs', 'tp'), may hold values from -0.125 to 0.125
- up_scale: float32 [4096], P('tp'), may hold values from 0.5 to 2
- down_weight: float32 [4096, 2048], P('tp', 'fs'), may hold values from -0.09375 to 0.09375
- down_scale: float32 [2048], P('fs'), may hold values from 0.3 to 3
- gain_ffn_out: float32 [2048], replicated, may hold values from 0.1 to 1.9
Outputs:
- result: bfloat16 [65536, 2048], P(('rep', 'fs'), 'tp')
All inputs are finite; a program needn't handle non-finite values.
Results may differ from a plain program's by a relative error of at most 0.013.
Values may be sent and summed in bfloat16 or wider, within the bound.
No kernel may reach another device: no remote copies, remote signals or barrier semaphores. Data moves between devices by JAX's collectives and lax.ppermute only.
A program may use at most 128 MiB of HBM per device.

v0:
```python
import jax
import jax.numpy as jnp
from jax import lax
from jax.sharding import PartitionSpec as P


def turned_gather(arrays, axis, dims):
    turned = [jnp.moveaxis(a, dim, 0) for a, dim in zip(arrays, dims)]
    widths = [t[0].size for t in turned]
    both = jnp.concatenate([t.reshape(-1, w) for t, w in zip(turned, widths)], axis=1)
    result = lax.all_gather(both, axis, axis=0, tiled=True)
    pieces = jnp.split(result, [sum(widths[:k]) for k in range(1, len(widths))], axis=1)
    return tuple(
        (
            jnp.moveaxis(b.reshape(-1, *t.shape[1:]), 0, dim)
            for b, t, dim in zip(pieces, turned, dims)
        )
    )


def in_one_piece(arrays, axis, dim, along):
    ends, at = ([], 0)
    for a in arrays[:-1]:
        at += a.shape[along]
        ends.append(at)
    both = jnp.concatenate(arrays, axis=along)
    return tuple(jnp.split(lax.all_gather(both, axis, axis=dim, tiled=True), ends, axis=along))


def copy_for_each(array, axis):
    copies = jnp.broadcast_to(array, (lax.axis_size(axis), *array.shape))
    return lax.all_to_all(copies, axis, split_axis=0, concat_axis=0, tiled=True)


def over_copies(array, axis):
    return copy_for_each(array, axis).sum(axis=0)


def packed_total(arrays, axis):
    vector, at, gathered = (jnp.concatenate([a.reshape(-1) for a in arrays]), 0, [])
    running = over_copies(vector, axis)
    for a in arrays:
        gathered.append(running[at : at + a.size].reshape(a.shape))
        at += a.size
    return tuple(gathered)


def in_order(pieces, dim):
    dims = list(pieces.shape[1:])
    dims[dim] *= pieces.shape[0]
    return jnp.moveaxis(pieces, 0, dim).reshape(dims)


def gathered_copies(array, axis, dim):
    pieces = copy_for_each(array, axis)
    return in_order(pieces, dim)


def total_of_pieces(array, axis):
    pieces = lax.all_gather(array, axis).astype(jnp.float32)
    return pieces.sum(axis=0)


def in_blocks(array, dim, peers):
    before, after = (array.shape[:dim], array.shape[dim + 1 :])
    return jnp.moveaxis(array.reshape(*before, peers, -1, *after), dim, 0)


def sent_and_summed(array, axis, dim):
    peers = lax.axis_size(axis)
    pieces = lax.all_to_all(in_blocks(array, dim, peers), axis, 0, 0, tiled=True)
    return jnp.sum(pieces.astype(jnp.float32), axis=0)


def rms_norm(values, gain, width, power_sum):
    return values * lax.rsqrt(power_sum / width + 1e-06) * gain


def local(
    resid,
    gain_mix_in,
    u_weight,
    v_weight,
    u_scale,
    v_scale,
    v_gain,
    mix_matrix,
    mix_bias,
    out_weight,
    out_scale,
    gain_mix_out,
    gain_ffn_in,
    up_weight,
    up_scale,
    down_weight,
    down_scale,
    gain_ffn_out,
):
    rows = resid.shape[0]
    part_width = resid.shape[1]
    width = part_width * lax.axis_size("tp")
    lane = lax.axis_index("tp")
    full_rows = lax.all_gather(resid, "tp", axis=1, tiled=True)
    out_scales, down_scales = turned_gather((out_scale, down_scale), "fs", (0, 0))
    full_float = full_rows.astype(jnp.float32)
    normed = rms_norm(
        full_float, gain_mix_in, width, jnp.sum(full_float * full_float, axis=1, keepdims=True)
    ).astype(jnp.bfloat16)
    branch_cols = u_weight.shape[1]
    pieces = in_one_piece(
        (u_weight.astype(jnp.bfloat16), v_weight.astype(jnp.bfloat16)), "fs", 0, 1
    )
    u_pre = jnp.dot(normed, pieces[0], preferred_element_type=jnp.float32)
    v_pre = jnp.dot(normed, pieces[1], preferred_element_type=jnp.float32)
    u_act = jax.nn.gelu(u_pre * u_scale)
    v_act = jax.nn.gelu(v_pre * v_scale)
    total, squares = packed_total(
        (jnp.sum(v_act, axis=1, keepdims=True), jnp.sum(v_act * v_act, axis=1, keepdims=True)), "tp"
    )
    branch_width = branch_cols * lax.axis_size("tp")
    centre = total / branch_width
    spread = squares / branch_width - centre * centre
    v_norm = ((v_act - centre) * lax.rsqrt(spread + 1e-06) * v_gain).astype(jnp.bfloat16)
    groups = mix_matrix.shape[0]
    block = mix_matrix.shape[1]
    blocks = v_norm.reshape(rows // block, block, groups, branch_cols // groups)
    mixed = (
        jnp.einsum(
            "gts,bsgd->btgd",
            mix_matrix.astype(jnp.bfloat16),
            blocks,
            preferred_element_type=jnp.float32,
        )
        + mix_bias.T[None, :, :, None]
    )
    gated = (u_act * mixed.reshape(rows, branch_cols)).astype(jnp.bfloat16)
    partial_value = jnp.dot(
        gated,
        gathered_copies(out_weight.astype(jnp.bfloat16), "fs", 1),
        preferred_element_type=jnp.float32,
    )
    mix_out = (
        total_of_pieces(partial_value.astype(jnp.bfloat16), "tp").astype(jnp.float32) * out_scales
    )
    power = jnp.sum(mix_out * mix_out, axis=1, keepdims=True)
    middle_full = (full_float + rms_norm(mix_out, gain_mix_out, width, power)).astype(jnp.bfloat16)
    middle = lax.dynamic_slice_in_dim(middle_full, lane * part_width, part_width, 1)
    middle_float = middle_full.astype(jnp.float32)
    ffn_in = rms_norm(
        middle_float,
        gain_ffn_in,
        width,
        jnp.sum(middle_float * middle_float, axis=1, keepdims=True),
    ).astype(jnp.bfloat16)
    up_half = up_weight.astype(jnp.bfloat16)
    down_half = down_weight.astype(jnp.bfloat16)
    whole_up = lax.all_gather(up_half, "fs", axis=0, tiled=True)
    raised = jnp.dot(ffn_in, whole_up, preferred_element_type=jnp.float32)
    hidden = jnp.square(jax.nn.relu(raised * up_scale)).astype(jnp.bfloat16)
    whole_down = lax.all_gather(down_half, "fs", axis=1, tiled=True)
    terms = jnp.dot(hidden, whole_down, preferred_element_type=jnp.float32)
    own_down = lax.dynamic_slice_in_dim(down_scales, lane * part_width, part_width, 0)
    ffn_out = sent_and_summed(terms.astype(jnp.bfloat16), "tp", 1) * own_down
    power_out = over_copies(jnp.sum(ffn_out * ffn_out, axis=1, keepdims=True), "tp")
    own_gain_out = lax.dynamic_slice_in_dim(gain_ffn_out, lane * part_width, part_width, 0)
    return (middle.astype(jnp.float32) + rms_norm(ffn_out, own_gain_out, width, power_out)).astype(
        jnp.bfloat16
    )


def solution(mesh):
    in_specs = (
        P(("rep", "fs"), "tp"),
        P(),
        P("fs", "tp"),
        P("fs", "tp"),
        P("tp"),
        P("tp"),
        P("tp"),
        P("tp", None, None),
        P("tp", None),
        P("tp", "fs"),
        P("fs"),
        P(),
        P(),
        P("fs", "tp"),
        P("tp"),
        P("tp", "fs"),
        P("fs"),
        P(),
    )
    out_specs = P(("rep", "fs"), "tp")
    return jax.shard_map(local, mesh=mesh, in_specs=in_specs, out_specs=out_specs, check_vma=False)
```

profile of v0, /device:TPU:1, one launch (start us, length us, event | category | flops | bytes accessed | tf_op | source)
XLA Modules:
  0.0 657.6 jit_solution(17726470480720936505)
XLA Ops:
  6.5 0.7 all-gather.8.cloned.1.call-update
  7.3 0.0 all-gather.10.cloned.1.call-start
  7.3 0.9 convert_element_type.62
  8.2 0.9 convert_element_type.63
  9.1 0.7 pad_maximum_fusion
  9.8 0.0 all-gather.10.cloned.1.call-update
  9.8 0.9 convert_element_type.67
  10.8 18.3 %all-gather.8.cloned.1.call-done = bf16[1024,2048]{1,0:T(8,128)(2,1)} async-done(((bf16[1024,1024]{1,0:T(8,128)(2,1)}), bf16[1024,2048]{1,0:T(8,128)(2,1)}) %all-gather.8.cloned.1.call-update) | async-done | bytes 4194320 | tf_op jit(solution)/shard_map/all_gather | solution.py:103
  29.0 3.1 fusion.3
  32.1 135.9 %all-gather.10.cloned.1.call-done = bf16[2048,1024]{1,0:T(8,128)(2,1)} async-done(((bf16[64,1024]{1,0:T(8,128)(2,1)}), bf16[2048,1024]{1,0:T(8,128)(2,1)}) %all-gather.10.cloned.1.call-update) | async-done | bytes 4194320 | tf_op jit(solution)/shard_map/all_gather | solution.py:27
  168.0 5.8 fusion.68
  173.8 24.0 %all_to_all.21 = f32[2,1,2048]{2,1,0:T(1,128)S(1)} all-to-all(f32[2,1,2048]{2,1,0:T(1,128)S(1)} %broadcast_in_dim.6), channel_id=1, replica_groups=mesh['rep'=2,'fs'=32,'tp'=2] {'tp'}, dimensions={0} | all-to-all | bytes 32768 | tf_op jit(solution)/shard_map/all_to_all | solution.py:32
  197.8 1.6 broadcast_in_dim.7
  199.4 7.1 %all-to-all-start.1 = ((bf16[32,512,64]{1,2,0:T(8,128)(2,1)}), bf16[32,512,64]{1,2,0:T(8,128)(2,1)}, u32[]{:S(2)}, u32[]{:S(2)}) async-start(bf16[32,512,64]{1,2,0:T(8,128)(2,1)} %broadcast_in_dim.7), calls=%async_computation.1 | async-start | bytes 4194304 | tf_op jit(solution)/shard_map/all_to_all | solution.py:32
  206.5 0.0 all-gather.16.cloned.1.call-start
  206.6 0.3 multiply_convert_fusion.1
  206.9 2.1 reshape.90
  209.1 2.4 bitcast_add_fusion
  211.5 2.7 copy.55
  214.2 3.4 reshape.91
  217.6 15.7 %all-to-all-done.1 = bf16[32,512,64]{1,2,0:T(8,128)(2,1)} async-done(((bf16[32,512,64]{1,2,0:T(8,128)(2,1)}), bf16[32,512,64]{1,2,0:T(8,128)(2,1)}, u32[]{:S(2)}, u32[]{:S(2)}) %all-to-all-start.1) | async-done | bytes 2097184 | tf_op jit(solution)/shard_map/all_to_all | solution.py:32
  233.4 10.3 %convolution_convert_fusion = bf16[1024,2048]{1,0:T(8,128)(2,1)} fusion(bf16[512,2048]{0,1:T(8,128)(2,1)} %bitcast.5, f32[1024,512]{1,0:T(8,128)S(1)} %reshape.91, bf16[2048,1024]{1,0:T(8,128)(2,1)} %all-gather.10.cloned.1.call-done, bf16[1024,2048]{1,0:T(8,128)(2,1)} %all-gather.8.cloned.1.call-done, f32[2048]{0:T(1024)S(1)} %copy-done.10, ...), kind=kOutput, calls=%fused_computation.24 | convolution fusion | flops 4311220224 | bytes 14694400 | tf_op jit(solution)/shard_map/dot_general | solution.py:137
  243.7 0.0 all-gather.16.cloned.1.call-update
  243.8 0.0 all-gather.12.cloned.1.call-start
  243.8 1.0 copy-done.3
  244.8 0.7 convert_element_type.74
  245.5 0.0 all-gather.12.cloned.1.call-update
  245.5 0.0 all-gather.14.cloned.1.call-start
  245.6 0.7 convert_element_type.76
  246.3 0.0 all-gather.14.cloned.1.call-update
  246.4 66.4 %all-gather.1 = f32[32,64,2]{1,2,0:T(2,128)S(1)} all-gather(f32[1,64,2]{1,2,0:T(2,128)S(1)} %maximum_bitcast_fusion), channel_id=1, replica_groups=mesh['rep'=2,'fs'=32,'tp'=2] {'fs'}, dimensions={0}, use_global_device_ids=true | all-gather | bytes 16896 | tf_op jit(solution)/shard_map/all_gather | solution.py:11
  312.8 0.1 reshape.88
  312.9 0.0 all-gather.16.cloned.1.call-done
  313.0 9.9 %convert_reduce_fusion = f32[1024,2048]{1,0:T(8,128)} fusion(bf16[2,1024,2048]{2,1,0:T(8,128)(2,1)} %bitcast.34), kind=kLoop, calls=%fused_computation | loop fusion | flops 6291456 | bytes 16777216 | tf_op jit(solution)/shard_map/reduce_sum | solution.py:61
  322.9 4.5 multiply_reduce_fusion
  327.5 1.3 copy-done
  328.8 4.0 fusion
  332.8 82.2 %all-gather.12.cloned.1.call-done = bf16[2048,2048]{1,0:T(8,128)(2,1)} async-done(((bf16[64,2048]{1,0:T(8,128)(2,1)}), bf16[2048,2048]{1,0:T(8,128)(2,1)}) %all-gather.12.cloned.1.call-update) | async-done | bytes 8388624 | tf_op jit(solution)/shard_map/all_gather | solution.py:157
  415.0 167.9 %all-gather.14.cloned.1.call-done = bf16[2048,2048]{0,1:T(8,128)(2,1)} async-done(((bf16[2048,64]{0,1:T(8,128)(2,1)}), bf16[2048,2048]{0,1:T(8,128)(2,1)}) %all-gather.14.cloned.1.call-update) | async-done | bytes 8388624 | tf_op jit(solution)/shard_map/all_gather | solution.py:160
  582.9 25.7 %fusion.16 = bf16[1024,2048]{1,0:T(8,128)(2,1)} fusion(bf16[2048,2048]{0,1:T(8,128)(2,1)} %all-gather.14.cloned.1.call-done, bf16[2048,2048]{1,0:T(8,128)(2,1)} %all-gather.12.cloned.1.call-done, bf16[1024,2048]{1,0:T(8,128)(2,1)} %get-tuple-element.8, f32[2048]{0:T(1024)S(1)} %copy-done.11, f32[2048]{0:T(1024)S(1)} %copy-done.12, f32[1024]{0:T(1024)S(1)} %add_rsqrt_fusion.1), kind=kOutput, calls=%fused_computation.25 | convolution fusion | flops 17198743552 | bytes 25186304 | tf_op jit(solution)/shard_map/dot_general | solution.py:161
  608.5 2.6 copy.66
  611.2 27.7 %all_to_all.22 = bf16[2,1024,1024]{2,1,0:T(8,128)(2,1)S(1)} all-to-all(bf16[2,1024,1024]{2,1,0:T(8,128)(2,1)S(1)} %bitcast.33), channel_id=1, replica_groups=mesh['rep'=2,'fs'=32,'tp'=2] {'tp'}, dimensions={0} | all-to-all | bytes 8388608 | tf_op jit(solution)/shard_map/all_to_all | solution.py:71
  638.8 1.0 convert_reduce_fusion.1
  639.9 0.0 dynamic-slice-start
  639.9 1.9 copy-done.1
  641.8 0.5 multiply_reduce_fusion.1
  642.3 3.7 all_to_all.23
  646.1 5.0 add_convert_fusion
  (43 shorter events, 0.2 us)
Async XLA Ops:
  6.5 161.5 %copy-start.10 = (f32[2048]{0:T(1024)S(1)}, f32[2048]{0:T(1024)}, u32[]{:S(2)}) copy-start(f32[2048]{0:T(1024)} %param.19) | copy-start | bytes 24580
  6.5 161.5 %copy-start.13 = (f32[512]{0:T(512)S(1)}, f32[512]{0:T(512)}, u32[]{:S(2)}) copy-start(f32[512]{0:T(512)} %param.23) | copy-start | bytes 6148
  6.5 22.5 %all-gather.8.cloned.1.call-start = ((), (), s32[]{:S(2)}) async-start(), calls=%async_computation.4 | async-start | bytes 6291456 | tf_op jit(solution)/shard_map/all_gather | solution.py:103
  7.3 160.7 %all-gather.10.cloned.1.call-start = ((), (), s32[]{:S(2)}) async-start(), calls=%async_computation.5 | async-start | bytes 4325376 | tf_op jit(solution)/shard_map/all_gather | solution.py:27
  173.8 32.8 %copy-start.7 = (f32[512]{0:T(512)S(1)}, f32[512]{0:T(512)}, u32[]{:S(2)}) copy-start(f32[512]{0:T(512)} %param.24) | copy-start | bytes 6148
  199.4 34.0 %all-to-all-start.1 = ((bf16[32,512,64]{1,2,0:T(8,128)(2,1)}), bf16[32,512,64]{1,2,0:T(8,128)(2,1)}, u32[]{:S(2)}, u32[]{:S(2)}) async-start(bf16[32,512,64]{1,2,0:T(8,128)(2,1)} %broadcast_in_dim.7), calls=%async_computation.1 | async-start | bytes 4194304 | tf_op jit(solution)/shard_map/all_to_all | solution.py:32
  206.5 2.6 copy-start.6
  206.5 106.5 %all-gather.16.cloned.1.call-start = ((), (), s32[]{:S(2)}) async-start(), calls=%async_computation.8 | async-start | bytes 12582912 | tf_op jit(solution)/shard_map/all_gather | solution.py:60
  214.2 19.2 %copy-start.14 = (f32[512]{0:T(512)S(1)}, f32[512]{0:T(512)}, u32[]{:S(2)}) copy-start(f32[512]{0:T(512)} %param.22) | copy-start | bytes 6148
  243.7 1.0 copy-start.3
  243.7 1.9 copy-start.4
  243.7 2.6 copy-start.8
  243.7 2.6 copy-start.9
  243.8 171.2 %all-gather.12.cloned.1.call-start = ((), (), s32[]{:S(2)}) async-start(), calls=%async_computation.6 | async-start | bytes 8650752 | tf_op jit(solution)/shard_map/all_gather | solution.py:157
  245.5 337.3 %all-gather.14.cloned.1.call-start = ((), (), s32[]{:S(2)}) async-start(), calls=%async_computation.7 | async-start | bytes 8650752 | tf_op jit(solution)/shard_map/all_gather | solution.py:160
  313.0 14.5 %copy-start.2 = (bf16[1024,2048]{1,0:T(8,128)(2,1)S(1)}, bf16[1024,2048]{1,0:T(8,128)(2,1)}, u32[]{:S(2)}) copy-start(bf16[1024,2048]{1,0:T(8,128)(2,1)} %all-gather.8.cloned.1.call-done) | copy-start | bytes 12582916
  322.9 5.9 copy-start
  322.9 5.9 copy-start.5
  328.8 254.1 %copy-start.11 = (f32[2048]{0:T(1024)S(1)}, f32[2048]{0:T(1024)}, u32[]{:S(2)}) copy-start(f32[2048]{0:T(1024)} %param.32) | copy-start | bytes 24580
  328.8 254.1 %copy-start.12 = (f32[2048]{0:T(1024)S(1)}, f32[2048]{0:T(1024)}, u32[]{:S(2)}) copy-start(f32[2048]{0:T(1024)} %param.30) | copy-start | bytes 24580
  639.9 1.9 copy-start.1
  639.9 6.2 dynamic-slice-start
Sparse Core Ops, SparseCore 0:
  9.0 19.9 all-gather.7
  30.7 137.2 all-gather.9
  243.9 22.8 all-gather.15
  268.3 146.6 all-gather.11
  416.4 166.3 all-gather.13
where the time goes:
time: 658 us
  waiting for transfers between devices  421 us (64%)
  blocking collectives  122 us (19%)
  matrix products  44.2 us (7%)
  other arithmetic  33.3 us (5%)
  local copies, waits for them, and re-layouts  16.9 us (3%)
  between operations  13.4 us (2%)
  starting transfers between devices  7.24 us (1%)
    all_gather x1, waiting for transfers between devices, local(): whole_down = lax.all_gather(down_half, 'fs', axis=1, tiled=True)  168 us
    all_gather x1, waiting for transfers between devices, in_one_piece(): lax.all_gather(both, axis, axis=dim, tiled=True)  136 us
    all_gather x1, waiting for transfers between devices, local(): whole_up = lax.all_gather(up_half, 'fs', axis=0, tiled=True)  82.2 us
    all_gather x1, blocking collectives, turned_gather(): result = lax.all_gather(both, axis, axis=0, tiled=True)  66.4 us
    all_to_all x2, blocking collectives, copy_for_each(): return lax.all_to_all(copies, axis, split_axis=0, concat_axis=0, tiled=True)  27.7 us
    all_to_all x1, blocking collectives, sent_and_summed(): lax.all_to_all(in_blocks(array, dim, peers), axis, 0, 0, tiled=True)  27.7 us
    dot_general x1, matrix products, local(): terms = jnp.dot(hidden, whole_down, preferred_element_type=jnp.float32)  25.7 us
    all_gather x1, waiting for transfers between devices, local(): full_rows = lax.all_gather(resid, 'tp', axis=1, tiled=True)  18.3 us
  transfers between devices with their start and end apart: 6, of which 5 were waited for; matrix products, arithmetic and copies ran while one was open for 6% of the time, Pallas kernels for 0%

commit v1 on v0

--- a/solution.py
+++ b/solution.py
@@ -157,7 +157,15 @@
     whole_up = lax.all_gather(up_half, "fs", axis=0, tiled=True)
     raised = jnp.dot(ffn_in, whole_up, preferred_element_type=jnp.float32)
     hidden = jnp.square(jax.nn.relu(raised * up_scale)).astype(jnp.bfloat16)
-    whole_down = lax.all_gather(down_half, "fs", axis=1, tiled=True)
+    whole_down = jnp.concatenate(
+        lax.all_to_all(
+            jnp.stack([down_half] * lax.axis_size("fs")),
+            axis_name="fs",
+            split_axis=0,
+            concat_axis=0,
+        ),
+        axis=1,
+    )
     terms = jnp.dot(hidden, whole_down, preferred_element_type=jnp.float32)
     own_down = lax.dynamic_slice_in_dim(down_scales, lane * part_width, part_width, 0)
     ffn_out = sent_and_summed(terms.astype(jnp.bfloat16), "tp", 1) * own_down

time: 658 us -> 554 us (0.84)
  waiting for transfers between devices: 421 us -> 176 us
  blocking collectives: 122 us -> 252 us
    all_gather x1 -> x0, waiting for transfers between devices: 168 us -> none  [local(): whole_down = lax.all_gather(down_half, 'fs', axis=1, tiled=True)]
    all_gather x1, blocking collectives: 66.4 us -> 203 us  [turned_gather(): result = lax.all_gather(both, axis, axis=0, tiled=True)]
    all_gather x1, waiting for transfers between devices: 82.2 us -> 5.68 us  [local(): whole_up = lax.all_gather(up_half, 'fs', axis=0, tiled=True)]
  transfers between devices with their start and end apart: 6 -> 6, of which waited for: 5 -> 4; matrix products, arithmetic and copies ran while one was open for 6% -> 7% of each run, Pallas kernels for 0% -> 0%
where the time goes in v1:
time: 554 us; the launch traced here: 553 us
  blocking collectives  252 us (45%)
  waiting for transfers between devices  176 us (32%)
  matrix products  44.2 us (8%)
  other arithmetic  32.6 us (6%)
  local copies, waits for them, and re-layouts  21.2 us (4%)
  starting transfers between devices  13.4 us (2%)
  between operations  13.4 us (2%)
    all_gather x1, blocking collectives, turned_gather(): result = lax.all_gather(both, axis, axis=0, tiled=True)  203 us
    all_gather x1, waiting for transfers between devices, in_one_piece(): lax.all_gather(both, axis, axis=dim, tiled=True)  136 us
    all_to_all x2, blocking collectives, copy_for_each(): return lax.all_to_all(copies, axis, split_axis=0, concat_axis=0, tiled=True)  27.7 us
    dot_general x1, matrix products, local(): terms = jnp.dot(hidden, whole_down, preferred_element_type=jnp.float32)  25.6 us
    all_to_all x1, blocking collectives, sent_and_summed(): lax.all_to_all(in_blocks(array, dim, peers), axis, 0, 0, tiled=True)  21.8 us
    all_gather x1, waiting for transfers between devices, local(): full_rows = lax.all_gather(resid, 'tp', axis=1, tiled=True)  18.3 us
    all_to_all x1, waiting for transfers between devices, copy_for_each(): return lax.all_to_all(copies, axis, split_axis=0, concat_axis=0, tiled=True)  15.7 us
  transfers between devices with their start and end apart: 6, of which 4 were waited for; matrix products, arithmetic and copies ran while one was open for 7% of the time, Pallas kernels for 0%

profile of v1, /device:TPU:1, one launch (start us, length us, event | category | flops | bytes accessed | tf_op | source)
XLA Modules:
  0.0 553.4 jit_solution(16448828899005166675)
XLA Ops:
  6.5 0.7 all-gather.7.cloned.1.call-update
  7.3 0.0 all-gather.9.cloned.1.call-start
  7.3 0.9 convert_element_type.62
  8.2 0.9 convert_element_type.63
  9.1 0.7 pad_maximum_fusion
  9.8 0.0 all-gather.9.cloned.1.call-update
  9.8 0.9 convert_element_type.67
  10.8 18.3 %all-gather.7.cloned.1.call-done = bf16[1024,2048]{1,0:T(8,128)(2,1)} async-done(((bf16[1024,1024]{1,0:T(8,128)(2,1)}), bf16[1024,2048]{1,0:T(8,128)(2,1)}) %all-gather.7.cloned.1.call-update) | async-done | bytes 4194320 | tf_op jit(solution)/shard_map/all_gather | solution.py:103
  29.0 3.1 fusion.3
  32.1 135.9 %all-gather.9.cloned.1.call-done = bf16[2048,1024]{1,0:T(8,128)(2,1)} async-done(((bf16[64,1024]{1,0:T(8,128)(2,1)}), bf16[2048,1024]{1,0:T(8,128)(2,1)}) %all-gather.9.cloned.1.call-update) | async-done | bytes 4194320 | tf_op jit(solution)/shard_map/all_gather | solution.py:27
  168.0 5.8 %fusion.68 = (f32[1024]{0:T(1024)S(1)}, f32[1024]{0:T(1024)S(1)}, f32[1024,512]{1,0:T(8,128)S(1)}) fusion(f32[512]{0:T(512)S(1)} %copy-done.13, bf16[2048,1024]{1,0:T(8,128)(2,1)} %all-gather.9.cloned.1.call-done, bf16[1024,2048]{1,0:T(8,128)(2,1)} %all-gather.7.cloned.1.call-done, f32[2048]{0:T(1024)S(1)} %copy-done.10, f32[1024]{0:T(1024)S(1)} %add_rsqrt_fusion.3), kind=kOutput, calls=%fused_computation.78 | convolution fusion | flops 2162161664 | bytes 8411136 | tf_op jit(solution)/shard_map/dot_general | solution.py:114
  173.8 0.0 copy-start.7
  173.8 24.0 %all_to_all.26 = f32[2,1,2048]{2,1,0:T(1,128)S(1)} all-to-all(f32[2,1,2048]{2,1,0:T(1,128)S(1)} %broadcast_in_dim.6), channel_id=1, replica_groups=mesh['rep'=2,'fs'=32,'tp'=2] {'tp'}, dimensions={0} | all-to-all | bytes 32768 | tf_op jit(solution)/shard_map/all_to_all | solution.py:32
  197.8 1.6 broadcast_in_dim.7
  199.4 7.1 %all-to-all-start.1 = ((bf16[32,512,64]{1,2,0:T(8,128)(2,1)}), bf16[32,512,64]{1,2,0:T(8,128)(2,1)}, u32[]{:S(2)}, u32[]{:S(2)}) async-start(bf16[32,512,64]{1,2,0:T(8,128)(2,1)} %broadcast_in_dim.7), calls=%async_computation.1 | async-start | bytes 4194304 | tf_op jit(solution)/shard_map/all_to_all | solution.py:32
  206.5 0.0 copy-start.6
  206.5 0.0 all-gather.13.cloned.1.call-start
  206.6 0.3 multiply_convert_fusion.1
  206.9 2.1 reshape.100
  209.1 2.4 bitcast_add_fusion
  211.5 2.7 copy.56
  214.2 3.4 reshape.101
  217.6 15.7 %all-to-all-done.1 = bf16[32,512,64]{1,2,0:T(8,128)(2,1)} async-done(((bf16[32,512,64]{1,2,0:T(8,128)(2,1)}), bf16[32,512,64]{1,2,0:T(8,128)(2,1)}, u32[]{:S(2)}, u32[]{:S(2)}) %all-to-all-start.1) | async-done | bytes 2097184 | tf_op jit(solution)/shard_map/all_to_all | solution.py:32
  233.4 10.4 %convolution_convert_fusion = bf16[1024,2048]{1,0:T(8,128)(2,1)} fusion(bf16[512,2048]{0,1:T(8,128)(2,1)} %bitcast.5, f32[1024,512]{1,0:T(8,128)S(1)} %reshape.101, bf16[2048,1024]{1,0:T(8,128)(2,1)} %all-gather.9.cloned.1.call-done, bf16[1024,2048]{1,0:T(8,128)(2,1)} %all-gather.7.cloned.1.call-done, f32[2048]{0:T(1024)S(1)} %copy-done.10, ...), kind=kOutput, calls=%fused_computation.24 | convolution fusion | flops 4311220224 | bytes 14694400 | tf_op jit(solution)/shard_map/dot_general | solution.py:137
  243.8 0.0 all-gather.13.cloned.1.call-update
  243.8 0.0 all-gather.11.cloned.1.call-start
  243.9 1.0 copy-done.3
  244.9 0.7 convert_element_type.74
  245.6 0.0 all-gather.11.cloned.1.call-update
  245.7 4.3 stack.2
  250.0 6.2 %all-to-all-start.2 = ((bf16[32,2048,64]{1,2,0:T(8,128)(2,1)}), bf16[32,2048,64]{1,2,0:T(8,128)(2,1)}, u32[]{:S(2)}, u32[]{:S(2)}) async-start(bf16[32,2048,64]{1,2,0:T(8,128)(2,1)} %stack.2), calls=%async_computation.2 | async-start | bytes 16777216 | tf_op jit(solution)/shard_map/all_to_all | solution.py:161
  256.2 202.8 %all-gather.1 = f32[32,64,2]{1,2,0:T(2,128)S(1)} all-gather(f32[1,64,2]{1,2,0:T(2,128)S(1)} %maximum_bitcast_fusion), channel_id=1, replica_groups=mesh['rep'=2,'fs'=32,'tp'=2] {'fs'}, dimensions={0}, use_global_device_ids=true | all-gather | bytes 16896 | tf_op jit(solution)/shard_map/all_gather | solution.py:11
  459.0 0.1 reshape.98
  459.1 0.0 all-gather.13.cloned.1.call-done
  459.2 9.9 %convert_reduce_fusion = f32[1024,2048]{1,0:T(8,128)} fusion(bf16[2,1024,2048]{2,1,0:T(8,128)(2,1)} %bitcast.37), kind=kLoop, calls=%fused_computation | loop fusion | flops 6291456 | bytes 16777216 | tf_op jit(solution)/shard_map/reduce_sum | solution.py:61
  469.1 4.5 multiply_reduce_fusion
  473.6 1.3 copy-done
  474.9 4.0 fusion
  478.9 5.7 %all-gather.11.cloned.1.call-done = bf16[2048,2048]{1,0:T(8,128)(2,1)} async-done(((bf16[64,2048]{1,0:T(8,128)(2,1)}), bf16[2048,2048]{1,0:T(8,128)(2,1)}) %all-gather.11.cloned.1.call-update) | async-done | bytes 8388624 | tf_op jit(solution)/shard_map/all_gather | solution.py:157
  484.6 25.6 %fusion.16 = bf16[1024,2048]{1,0:T(8,128)(2,1)} fusion(bf16[2048,2048]{0,1:T(8,128)(2,1)} %bitcast.12, bf16[2048,2048]{1,0:T(8,128)(2,1)} %all-gather.11.cloned.1.call-done, bf16[1024,2048]{1,0:T(8,128)(2,1)} %get-tuple-element.8, f32[2048]{0:T(1024)S(1)} %copy-done.11, f32[2048]{0:T(1024)S(1)} %copy-done.12, f32[1024]{0:T(1024)S(1)} %add_rsqrt_fusion.1), kind=kOutput, calls=%fused_computation.25 | convolution fusion | flops 17198743552 | bytes 25186304 | tf_op jit(solution)/shard_map/dot_general | solution.py:169
  510.2 2.6 copy.67
  512.9 21.8 %all_to_all.27 = bf16[2,1024,1024]{2,1,0:T(8,128)(2,1)S(1)} all-to-all(bf16[2,1024,1024]{2,1,0:T(8,128)(2,1)S(1)} %bitcast.36), channel_id=1, replica_groups=mesh['rep'=2,'fs'=32,'tp'=2] {'tp'}, dimensions={0} | all-to-all | bytes 8388608 | tf_op jit(solution)/shard_map/all_to_all | solution.py:71
  534.6 1.0 convert_reduce_fusion.1
  535.7 0.0 dynamic-slice-start
  535.7 1.9 copy-done.1
  537.6 0.5 multiply_reduce_fusion.1
  538.1 3.7 all_to_all.28
  541.9 5.0 add_convert_fusion
  (43 shorter events, 0.2 us)
Async XLA Ops:
  6.5 161.5 %copy-start.10 = (f32[2048]{0:T(1024)S(1)}, f32[2048]{0:T(1024)}, u32[]{:S(2)}) copy-start(f32[2048]{0:T(1024)} %param.19) | copy-start | bytes 24580
  6.5 161.5 %copy-start.13 = (f32[512]{0:T(512)S(1)}, f32[512]{0:T(512)}, u32[]{:S(2)}) copy-start(f32[512]{0:T(512)} %param.23) | copy-start | bytes 6148
  6.5 22.5 %all-gather.7.cloned.1.call-start = ((), (), s32[]{:S(2)}) async-start(), calls=%async_computation.5 | async-start | bytes 6291456 | tf_op jit(solution)/shard_map/all_gather | solution.py:103
  7.3 160.7 %all-gather.9.cloned.1.call-start = ((), (), s32[]{:S(2)}) async-start(), calls=%async_computation.6 | async-start | bytes 4325376 | tf_op jit(solution)/shard_map/all_gather | solution.py:27
  173.8 32.8 %copy-start.7 = (f32[512]{0:T(512)S(1)}, f32[512]{0:T(512)}, u32[]{:S(2)}) copy-start(f32[512]{0:T(512)} %param.24) | copy-start | bytes 6148
  199.4 34.0 %all-to-all-start.1 = ((bf16[32,512,64]{1,2,0:T(8,128)(2,1)}), bf16[32,512,64]{1,2,0:T(8,128)(2,1)}, u32[]{:S(2)}, u32[]{:S(2)}) async-start(bf16[32,512,64]{1,2,0:T(8,128)(2,1)} %broadcast_in_dim.7), calls=%async_computation.1 | async-start | bytes 4194304 | tf_op jit(solution)/shard_map/all_to_all | solution.py:32
  206.5 2.6 copy-start.6
  206.5 252.7 %all-gather.13.cloned.1.call-start = ((), (), s32[]{:S(2)}) async-start(), calls=%async_computation.8 | async-start | bytes 12582912 | tf_op jit(solution)/shard_map/all_gather | solution.py:60
  214.2 19.2 %copy-start.14 = (f32[512]{0:T(512)S(1)}, f32[512]{0:T(512)}, u32[]{:S(2)}) copy-start(f32[512]{0:T(512)} %param.22) | copy-start | bytes 6148
  243.8 1.0 copy-start.3
  243.8 1.8 copy-start.4
  243.8 240.8 %all-gather.11.cloned.1.call-start = ((), (), s32[]{:S(2)}) async-start(), calls=%async_computation.7 | async-start | bytes 8650752 | tf_op jit(solution)/shard_map/all_gather | solution.py:157
  250.0 6.2 %copy-start.8 = (f32[64]{0:T(128)S(1)}, f32[64]{0:T(128)}, u32[]{:S(2)}) copy-start(f32[64]{0:T(128)} %param.34) | copy-start | bytes 772
  250.0 6.2 %copy-start.9 = (f32[64]{0:T(128)S(1)}, f32[64]{0:T(128)}, u32[]{:S(2)}) copy-start(f32[64]{0:T(128)} %param.28) | copy-start | bytes 772
  250.0 229.0 %all-to-all-start.2 = ((bf16[32,2048,64]{1,2,0:T(8,128)(2,1)}), bf16[32,2048,64]{1,2,0:T(8,128)(2,1)}, u32[]{:S(2)}, u32[]{:S(2)}) async-start(bf16[32,2048,64]{1,2,0:T(8,128)(2,1)} %stack.2), calls=%async_computation.2 | async-start | bytes 16777216 | tf_op jit(solution)/shard_map/all_to_all | solution.py:161
  459.2 14.4 %copy-start.2 = (bf16[1024,2048]{1,0:T(8,128)(2,1)S(1)}, bf16[1024,2048]{1,0:T(8,128)(2,1)}, u32[]{:S(2)}) copy-start(bf16[1024,2048]{1,0:T(8,128)(2,1)} %all-gather.7.cloned.1.call-done) | copy-start | bytes 12582916
  469.1 5.9 %copy-start = (f32[1024,2048]{1,0:T(8,128)S(1)}, f32[1024,2048]{1,0:T(8,128)}, u32[]{:S(2)}) copy-start(f32[1024,2048]{1,0:T(8,128)} %convert_reduce_fusion) | copy-start | bytes 25165828
  469.1 5.9 %copy-start.5 = (f32[2048]{0:T(1024)S(1)}, f32[2048]{0:T(1024)}, u32[]{:S(2)}) copy-start(f32[2048]{0:T(1024)} %param.29) | copy-start | bytes 24580
  474.9 9.7 %copy-start.11 = (f32[2048]{0:T(1024)S(1)}, f32[2048]{0:T(1024)}, u32[]{:S(2)}) copy-start(f32[2048]{0:T(1024)} %param.32) | copy-start | bytes 24580
  474.9 9.7 %copy-start.12 = (f32[2048]{0:T(1024)S(1)}, f32[2048]{0:T(1024)}, u32[]{:S(2)}) copy-start(f32[2048]{0:T(1024)} %param.30) | copy-start | bytes 24580
  535.7 1.9 copy-start.1
  535.7 6.2 %dynamic-slice-start = ((f32[2048]{0:T(1024)}, s32[]{:T(128)}), f32[1024]{0:T(1024)S(1)}, s32[]{:S(2)}) async-start(f32[2048]{0:T(1024)} %param.35, s32[]{:T(128)} %select_n.2), calls=%async_computation.9 | async-start | bytes 8704 | tf_op jit(solution)/shard_map/dynamic_slice | solution.py:173
Sparse Core Ops, SparseCore 0:
  9.0 19.9 all-gather.6
  30.7 137.2 all-gather.8
  244.0 22.8 all-gather.12
  268.3 216.2 all-gather.10
